TPU v7x, 32 devices: a whole 2x2x4 slice. The times are simulated.
32 devices in a mesh: kv: 8 (over z, y), tp: 4 (over x, core).
Axes of the slice: x: 2, y: 2, z: 4, core: 2. Of those that a mesh axis runs over, the one named last changes fastest.
Arguments:
- tokens: bfloat16 [128, 4096], P(None, 'kv'), may hold values from -152 to 152, as said below
- norm_gain: float32 [4096], P('kv'), may hold values from 0.1 to 1.9
- w_query: bfloat16 [4096, 2048], P('kv', 'tp'), may hold values from -0.09375 to 0.09375
- w_key: bfloat16 [4096, 2048], P('kv', 'tp'), may hold values from -0.375 to 0.375
- w_value: bfloat16 [4096, 2048], P('kv', 'tp'), may hold values from -0.09375 to 0.09375
- lambdas: float32 [16], P('tp'), may hold values from 0.3 to 0.8
- head_gain: float32 [128], replicated, may hold values from 0.1 to 1.9
- w_out: bfloat16 [2048, 4096], P('tp', 'kv'), may hold values from -0.125 to 0.125
- cache_keys: bfloat16 [8, 4096, 16, 128], P(None, 'kv', 'tp'), may hold values from -370 to 370
- cache_values: bfloat16 [8, 4096, 16, 128], P(None, 'kv', 'tp'), may hold values from -6 to 6
- lengths: int32 [8], replicated, may hold values from 2560 to 4074
- accepted: int32 [8], replicated, may hold values from 0 to 6
- parents: int32 [8, 16], replicated, may hold values from -1 to 14, as said below
Outputs:
- layer_out: bfloat16 [128, 4096], P('tp', 'kv')
- keys_out: bfloat16 [8, 4096, 16, 128], P(None, 'kv', 'tp')
- values_out: bfloat16 [8, 4096, 16, 128], P(None, 'kv', 'tp')
Inputs may be any that keep to these rules, and one draw needn't show every extreme that they name: `tokens`: columns of features have scales that differ; rows too. The proposals of the last step that were kept already stand right after the first lengths positions; the next 16 positions receive this step's proposals. `parents`: proposal 0 of every sequence has parent -1; every other proposal's parent is an earlier proposal of the same sequence, and the last proposal's parent is the one right before it.
All inputs are finite; a program needn't handle non-finite values.
Results may differ from a plain program's by a relative error of at most 0.015.
The roundings to bfloat16 on the way count: a program that leaves them out, or rounds other values in their place, can miss the bound.
Values may be sent and summed in bfloat16 or wider, within the bound.
A program may use at most 64 MiB of HBM per device.

v0:
```python
import jax
import jax.numpy as jnp
from jax import lax
from jax.sharding import PartitionSpec as P

D = 4096
HEAD = 64
KDIM = 128
PROP = 16


eps_row = 1e-06
eps_head = 1e-05
masked = -1e30


def ancestry(parents):
    members = parents.shape[0]
    indices = jnp.arange(members, dtype=jnp.int32)
    reachable = (parents[:, None] == indices[None, :]).astype(jnp.float32) + jnp.eye(
        members, dtype=jnp.float32
    )
    for repeat in range(max(1, (members - 1).bit_length())):
        reachable = jnp.minimum(jnp.dot(reachable, reachable, precision=lax.Precision.HIGHEST), 1.0)
    return reachable


def combine(earlier, latter):
    maxima_a, totals_a, summed_a = earlier
    maxima_b, totals_b, summed_b = latter
    highest = jnp.maximum(maxima_a, maxima_b)
    factor_a = jnp.exp(maxima_a - highest)
    factor_b = jnp.exp(maxima_b - highest)
    return (
        highest,
        totals_a * factor_a + totals_b * factor_b,
        summed_a * factor_a[..., None] + summed_b * factor_b[..., None],
    )


def softmax_block(scores, allowed, values):
    scores = jnp.where(allowed, scores, masked)
    maxima = jnp.max(scores, axis=-1)
    weights = jnp.where(allowed, jnp.exp(scores - maxima[..., None]), 0.0)
    totals = jnp.sum(weights, axis=-1)
    summed = jnp.einsum(
        "bjhmp,bphd->bjhmd",
        weights.astype(jnp.bfloat16),
        values,
        preferred_element_type=jnp.float32,
    )
    return (maxima, totals, summed)


def finish(merged, lambdas, head_gain):
    maxima, totals, summed = merged
    attended = summed / totals[..., None]
    blended = attended[..., 0, :] - lambdas[:, None] * attended[..., 1, :]
    inverse_rms = lax.rsqrt(jnp.mean(blended * blended, axis=-1, keepdims=True) + eps_head)
    return (blended * inverse_rms * head_gain).astype(jnp.bfloat16)


def leading(array, token_count):
    return array.reshape((1, token_count) + array.shape[2:])


def body(
    tokens,
    norm_gain,
    w_query,
    w_key,
    w_value,
    lambdas,
    head_gain,
    w_out,
    cache_keys,
    cache_values,
    lengths,
    accepted,
    parents,
):
    token_count = tokens.shape[0]
    sequences = token_count // PROP
    local_heads = w_query.shape[1] // KDIM
    widened = tokens.astype(jnp.float32)
    squares_local = jnp.sum(widened * widened, axis=1, keepdims=True)
    scaled = (widened * norm_gain[None, :]).astype(jnp.bfloat16)
    part_query = jnp.dot(scaled, w_query, preferred_element_type=jnp.float32)
    part_key = jnp.dot(scaled, w_key, preferred_element_type=jnp.float32)
    part_value = jnp.dot(scaled, w_value, preferred_element_type=jnp.float32)
    sum_query, sum_key, sum_value, squares = lax.psum(
        (part_query, part_key, part_value, squares_local), "kv"
    )
    row_scale = lax.rsqrt(squares / D + eps_row)
    queries = (row_scale * sum_query).astype(jnp.bfloat16)
    new_keys = (row_scale * sum_key).astype(jnp.bfloat16)
    new_values = (row_scale * sum_value).astype(jnp.bfloat16)
    query_pairs = queries.reshape(sequences, PROP, local_heads, 2, HEAD)
    key_pairs = new_keys.reshape(sequences, PROP, local_heads, 2, HEAD)
    keys_fresh = new_keys.reshape(sequences, PROP, local_heads, KDIM)
    values_fresh = new_values.reshape(sequences, PROP, local_heads, KDIM)
    cache_positions = cache_keys.shape[1]
    positions = lax.axis_index("kv") * cache_positions + jnp.arange(
        cache_positions, dtype=jnp.int32
    )
    limits = lengths + accepted
    usable = (positions[None, :] < limits[:, None])[:, None, None, None, :]
    score_scale = HEAD ** (-0.5)
    stored_pairs = cache_keys.reshape(sequences, cache_positions, local_heads, 2, HEAD)
    scores = (
        jnp.einsum(
            "bjhmd,bphmd->bjhmp", query_pairs, stored_pairs, preferred_element_type=jnp.float32
        )
        * score_scale
    )
    cache_part = softmax_block(scores, usable, cache_values)
    reachable = jax.vmap(ancestry)(parents) > 0.5
    tree_scores = (
        jnp.einsum("bjhmd,bihmd->bjhmi", query_pairs, key_pairs, preferred_element_type=jnp.float32)
        * score_scale
    )
    tree_part = softmax_block(tree_scores, reachable[:, :, None, None, :], values_fresh)
    own_rows = token_count // lax.axis_size("kv")
    first_row = lax.axis_index("kv") * own_rows
    arrived_max, arrived_totals, arrived_sums = (
        lax.all_to_all(
            leading(cache_part[0], token_count), "kv", split_axis=1, concat_axis=0, tiled=True
        ),
        lax.all_to_all(
            leading(cache_part[1], token_count), "kv", split_axis=1, concat_axis=0, tiled=True
        ),
        lax.all_to_all(
            leading(cache_part[2], token_count), "kv", split_axis=1, concat_axis=0, tiled=True
        ),
    )
    highest = jnp.max(arrived_max, axis=0)
    factors = jnp.exp(arrived_max - highest[None])
    folded = (
        highest,
        jnp.sum(arrived_totals * factors, axis=0),
        jnp.sum(arrived_sums * factors[..., None], axis=0),
    )
    own_tree = tuple(
        (
            lax.dynamic_slice_in_dim(
                member.reshape((token_count,) + member.shape[2:]), first_row, own_rows, 0
            )
            for member in tree_part
        )
    )
    finished = finish(combine(folded, own_tree), lambdas, head_gain).reshape(
        own_rows, local_heads * KDIM
    )
    normed = lax.all_gather(finished, "kv", axis=0, tiled=True)
    layer_out = lax.psum_scatter(
        jnp.dot(normed, w_out, preferred_element_type=jnp.float32).astype(jnp.bfloat16),
        "tp",
        scatter_dimension=0,
        tiled=True,
    )
    slot_of = positions[None, :, None] - limits[:, None, None]
    placing = (slot_of == jnp.arange(PROP, dtype=jnp.int32)[None, None, :]).astype(jnp.bfloat16)
    written = (jnp.sum(placing.astype(jnp.float32), axis=2) > 0.5)[:, :, None, None]
    placed_keys = jnp.einsum(
        "bpj,bjhd->bphd", placing, keys_fresh, preferred_element_type=jnp.float32
    ).astype(jnp.bfloat16)
    placed_values = jnp.einsum(
        "bpj,bjhd->bphd", placing, values_fresh, preferred_element_type=jnp.float32
    ).astype(jnp.bfloat16)
    keys_out = jnp.where(written, placed_keys, cache_keys)
    values_out = jnp.where(written, placed_values, cache_values)
    return (layer_out, keys_out, values_out)


def solution(mesh):
    return jax.shard_map(
        body,
        mesh=mesh,
        in_specs=(
            P(None, "kv"),
            P("kv"),
            P("kv", "tp"),
            P("kv", "tp"),
            P("kv", "tp"),
            P("tp"),
            P(),
            P("tp", "kv"),
            P(None, "kv", "tp", None),
            P(None, "kv", "tp", None),
            P(),
            P(),
            P(),
        ),
        out_specs=(P("tp", "kv"), P(None, "kv", "tp", None), P(None, "kv", "tp", None)),
        check_vma=False,
    )
```

profile of v0, /device:TPU:0, one launch (start us, length us, event | category | flops | bytes accessed | tf_op | source)
XLA Modules:
  0.0 199.4 jit_solution(11030734350312015369)
XLA Ops:
  7.2 1.1 copy-done
  8.4 1.9 fusion.40
  10.2 2.1 %fusion.42 = f32[128,512]{1,0:T(8,128)} fusion(bf16[512,512]{1,0:T(8,128)(2,1)} %param.16, bf16[128,512]{1,0:T(8,128)(2,1)} %param.13, f32[512]{0:T(512)} %param.14), kind=kOutput, calls=%fused_computation.56 | convolution fusion | flops 67305472 | bytes 919552 | tf_op jit(solution)/shard_map/dot_general | solution.py:89
  12.3 1.9 fusion.44
  14.3 23.6 %psum.28 = f32[128,1]{0,1:T(1,128)S(1)} all-reduce(f32[128,1]{0,1:T(1,128)S(1)} %bitcast.101), channel_id=1, replica_groups=mesh['kv'=8,'tp'=4] {'kv'}, use_global_device_ids=true, to_apply=%region_1.0 | all-reduce | flops 128 | bytes 1024 | tf_op jit(solution)/shard_map/psum | solution.py:91
  38.0 7.5 %copy.156 = bf16[8,512,4,128]{1,3,2,0:T(8,128)(2,1)} copy(bf16[8,512,4,128]{3,2,1,0:T(4,128)(2,1)} %param.21) | data formatting | bytes 8388608 | tf_op args[8]
  46.6 0.7 broadcast_bitcast_fusion
  47.4 0.6 broadcast_compare_fusion
  48.0 44.8 %all-reduce.3.cloned.1.call-done = (f32[128,512]{1,0:T(8,128)}, f32[128,512]{1,0:T(8,128)}, f32[128,512]{1,0:T(8,128)}) async-done(((f32[128,512]{1,0:T(8,128)}, f32[128,512]{1,0:T(8,128)}, f32[128,512]{1,0:T(8,128)}), (f32[128,512]{1,0:T(8,128)}, f32[128,512]{1,0:T(8,128)}, f32[128,512]{1,0:T(8,128)})) %all-reduce.3.cloned.1.call-update) | async-done | bytes 786448 | tf_op jit(solution)/shard_map/psum | solution.py:91
  92.8 1.2 multiply_convert_fusion
  94.2 3.0 %bitcast_reduce_fusion = (f32[8,16,4,2]{1,3,2,0:T(2,128)S(1)}, f32[8,4,2,16,512]{4,3,2,1,0:T(8,128)S(1)}) fusion(pred[8,512]{1,0:T(8,128)(4,1)S(1)} %broadcast_compare_fusion.1, bf16[8,512,4,2,64]{1,4,3,2,0:T(8,128)(2,1)} %bitcast.84, bf16[8,16,4,2,64]{4,3,2,1,0:T(2,128)(2,1)S(1)} %reshape.160), kind=kOutput, calls=%fused_computation.5 | convolution fusion | flops 68680704 | bytes 6430720 | tf_op jit(solution)/shard_map/bjhmd,bphmd->bjhmp/dot_general | solution.py:111
  97.2 0.7 fusion.4
  98.2 0.8 reshape.183
  99.0 3.9 %all-to-all-start.2 = ((f32[8,1,128]{2,1,0:T(1,128)}), f32[8,1,128]{2,1,0:T(1,128)}, u32[]{:S(2)}, u32[]{:S(2)}) async-start(f32[8,1,128]{2,1,0:T(1,128)} %reshape.183), calls=%async_computation.2 | async-start | bytes 8192 | tf_op jit(solution)/shard_map/all_to_all | solution.py:129
  103.1 4.0 %fusion.6 = f32[8,16,4,2,128]{4,1,3,2,0:T(8,128)} fusion(bf16[8,512,4,128,1]{3,2,1,0,4:T(4,128)(2,1)} %bitcast.102, f32[8,4,2,16,512]{4,3,2,1,0:T(8,128)S(1)} %get-tuple-element.41, f32[8,16,4,2]{1,3,2,0:T(2,128)S(1)} %get-tuple-element.40, pred[8,512]{1,0:T(8,128)(4,1)S(1)} %broadcast_compare_fusion.1), kind=kOutput, calls=%fused_computation.12 | convolution fusion | flops 136839168 | bytes 6823936 | tf_op jit(solution)/shard_map/bjhmp,bphd->bjhmd/dot_general | solution.py:46
  108.0 0.8 reshape.181
  109.3 5.4 %all-to-all-start.1 = ((f32[8,1,128]{2,1,0:T(1,128)}), f32[8,1,128]{2,1,0:T(1,128)S(1)}, u32[]{:S(2)}, u32[]{:S(2)}) async-start(f32[8,1,128]{2,1,0:T(1,128)} %reshape.181), calls=%async_computation.1 | async-start | bytes 8192 | tf_op jit(solution)/shard_map/all_to_all | solution.py:126
  114.9 1.0 copy.200
  116.3 1.2 copy.160
  117.5 3.6 %all-to-all-done.1 = f32[8,1,128]{2,1,0:T(1,128)S(1)} async-done(((f32[8,1,128]{2,1,0:T(1,128)}), f32[8,1,128]{2,1,0:T(1,128)S(1)}, u32[]{:S(2)}, u32[]{:S(2)}) %all-to-all-start.1) | async-done | bytes 4128 | tf_op jit(solution)/shard_map/all_to_all | solution.py:126
  121.2 3.5 %all-to-all-start = ((f32[1,128,4,2,128]{4,3,2,0,1:T(2,128)}), f32[1,128,4,2,128]{4,3,2,0,1:T(2,128)S(1)}, u32[]{:S(2)}, u32[]{:S(2)}) async-start(f32[1,128,4,2,128]{4,3,2,0,1:T(2,128)} %copy.160), calls=%async_computation | async-start | bytes 1048576 | tf_op jit(solution)/shard_map/all_to_all | solution.py:132
  124.9 3.6 %copy_select_fusion.1 = bf16[8,512,4,128]{3,1,2,0:T(8,128)(2,1)S(1)} fusion(bf16[8,512,4,128]{3,2,1,0:T(4,128)(2,1)} %param.21, pred[8,512]{1,0:T(8,128)(4,1)S(1)} %copy-done.12, bf16[8,16,4,128]{3,2,1,0:T(4,128)(2,1)S(1)} %reshape.170, s32[8,512]{1,0:T(8,128)S(1)} %copy-done.8), kind=kOutput, calls=%fused_computation.3 | convolution fusion | flops 71368704 | bytes 8540160 | tf_op jit(solution)/shard_map/bpj,bjhd->bphd/dot_general | solution.py:164
  128.5 5.3 %copy.189 = bf16[8,512,4,128]{3,2,1,0:T(4,128)(2,1)} copy(bf16[8,512,4,128]{3,1,2,0:T(8,128)(2,1)S(1)} %copy_select_fusion.1) | data formatting | bytes 8388608
  134.3 0.7 reduce.5
  135.7 1.3 reduce.4
  137.9 0.8 multiply_add_fusion
  138.7 0.7 multiply_reduce_fusion
  140.2 30.8 %all_gather.3 = bf16[128,512]{1,0:T(8,128)(2,1)S(1)} all-gather(bf16[16,512]{1,0:T(8,128)(2,1)S(1)} %fusion.53), channel_id=1, replica_groups=mesh['kv'=8,'tp'=4] {'kv'}, dimensions={0}, use_global_device_ids=true | all-gather | bytes 147456 | tf_op jit(solution)/shard_map/all_gather | solution.py:154
  171.0 0.9 convolution_convert_fusion
  171.9 3.5 %copy_select_fusion = bf16[8,512,4,128]{3,1,2,0:T(8,128)(2,1)S(1)} fusion(bf16[8,512,4,128]{3,2,1,0:T(4,128)(2,1)} %param.22, pred[8,512]{1,0:T(8,128)(4,1)S(1)} %copy-done.12, bf16[8,16,4,128]{3,2,1,0:T(4,128)(2,1)S(1)} %reshape.166, s32[8,512]{1,0:T(8,128)S(1)} %copy-done.8), kind=kOutput, calls=%fused_computation.2 | convolution fusion | flops 71368704 | bytes 8540160 | tf_op jit(solution)/shard_map/bpj,bjhd->bphd/dot_general | solution.py:167
  175.5 5.3 %copy.190 = bf16[8,512,4,128]{3,2,1,0:T(4,128)(2,1)} copy(bf16[8,512,4,128]{3,1,2,0:T(8,128)(2,1)S(1)} %copy_select_fusion) | data formatting | bytes 8388608
  180.7 11.8 %reduce-scatter.2.cloned.1.call-done = bf16[32,512]{1,0:T(8,128)(2,1)} async-done(((bf16[128,512]{1,0:T(8,128)(2,1)}), bf16[32,512]{1,0:T(8,128)(2,1)}) %reduce-scatter.2.cloned.1.call-update) | async-done | bytes 32784 | tf_op jit(solution)/shard_map/reduce_scatter | solution.py:155
  (84 shorter events, 7.0 us)
Async XLA Ops:
  7.2 1.2 copy-start
  7.2 7.0 %copy-start.1 = (bf16[128,512]{1,0:T(8,128)(2,1)S(1)}, bf16[128,512]{1,0:T(8,128)(2,1)}, u32[]{:S(2)}) copy-start(bf16[128,512]{1,0:T(8,128)(2,1)} %param.13) | copy-start | bytes 393220
  7.2 5.1 %copy-start.2 = (bf16[512,512]{1,0:T(8,128)(2,1)S(1)}, bf16[512,512]{1,0:T(8,128)(2,1)}, u32[]{:S(2)}) copy-start(bf16[512,512]{1,0:T(8,128)(2,1)} %param.15) | copy-start | bytes 1572868
  7.2 85.6 %all-reduce.3.cloned.1.call-start = ((), (), s32[]{:S(2)}) async-start(), calls=%async_computation.5 | async-start | bytes 1572864 | tf_op jit(solution)/shard_map/psum | solution.py:91
  38.0 7.5 %copy-start.11 = (s32[8,16]{1,0:T(8,128)S(1)}, s32[8,16]{1,0:T(8,128)}, u32[]{:S(2)}) copy-start(s32[8,16]{1,0:T(8,128)} %param.25) | copy-start | bytes 1540
  38.0 8.5 %copy-start.16 = (s32[8]{0:T(128)S(1)}, s32[8]{0:T(128)}, u32[]{:S(2)}) copy-start(s32[8]{0:T(128)} %param.23) | copy-start | bytes 100
  38.0 8.5 %copy-start.17 = (s32[8]{0:T(128)S(1)}, s32[8]{0:T(128)}, u32[]{:S(2)}) copy-start(s32[8]{0:T(128)} %param.24) | copy-start | bytes 100
  38.0 8.6 %copy-start.13 = (f32[4]{0:T(128)S(1)}, f32[4]{0:T(128)}, u32[]{:S(2)}) copy-start(f32[4]{0:T(128)} %param.18) | copy-start | bytes 52
  38.0 8.6 %copy-start.15 = (f32[128]{0:T(128)S(1)}, f32[128]{0:T(128)}, u32[]{:S(2)}) copy-start(f32[128]{0:T(128)} %param.19) | copy-start | bytes 1540
  46.5 47.7 %copy-start.7 = (s32[8,512]{1,0:T(8,128)}, s32[8,512]{1,0:T(8,128)S(1)}, u32[]{:S(2)}) copy-start(s32[8,512]{1,0:T(8,128)S(1)} %broadcast_subtract_fusion) | copy-start | bytes 49156
  97.2 9.9 %copy-start.5 = (f32[8,16,4,2]{1,3,2,0:T(2,128)}, f32[8,16,4,2]{1,3,2,0:T(2,128)S(1)}, u32[]{:S(2)}) copy-start(f32[8,16,4,2]{1,3,2,0:T(2,128)S(1)} %get-tuple-element.40) | copy-start | bytes 12292
  99.0 10.3 %all-to-all-start.2 = ((f32[8,1,128]{2,1,0:T(1,128)}), f32[8,1,128]{2,1,0:T(1,128)}, u32[]{:S(2)}, u32[]{:S(2)}) async-start(f32[8,1,128]{2,1,0:T(1,128)} %reshape.183), calls=%async_computation.2 | async-start | bytes 8192 | tf_op jit(solution)/shard_map/all_to_all | solution.py:129
  107.1 0.8 copy-start.6
  107.1 9.1 %copy-start.4 = (f32[8,16,4,2,128]{4,1,3,2,0:T(8,128)S(1)}, f32[8,16,4,2,128]{4,1,3,2,0:T(8,128)}, u32[]{:S(2)}) copy-start(f32[8,16,4,2,128]{4,1,3,2,0:T(8,128)} %fusion.6) | copy-start | bytes 1572868
  109.3 11.9 %all-to-all-start.1 = ((f32[8,1,128]{2,1,0:T(1,128)}), f32[8,1,128]{2,1,0:T(1,128)S(1)}, u32[]{:S(2)}, u32[]{:S(2)}) async-start(f32[8,1,128]{2,1,0:T(1,128)} %reshape.181), calls=%async_computation.1 | async-start | bytes 8192 | tf_op jit(solution)/shard_map/all_to_all | solution.py:126
  116.2 8.7 %copy-start.8 = (s32[8,512]{1,0:T(8,128)S(1)}, s32[8,512]{1,0:T(8,128)}, u32[]{:S(2)}) copy-start(s32[8,512]{1,0:T(8,128)} %copy-done.7) | copy-start | bytes 49156
  116.2 8.7 %copy-start.12 = (pred[8,512]{1,0:T(8,128)(4,1)S(1)}, pred[8,512]{1,0:T(8,128)(4,1)}, u32[]{:S(2)}) copy-start(pred[8,512]{1,0:T(8,128)(4,1)} %broadcast_compare_fusion) | copy-start | bytes 12292
  121.2 17.6 %all-to-all-start = ((f32[1,128,4,2,128]{4,3,2,0,1:T(2,128)}), f32[1,128,4,2,128]{4,3,2,0,1:T(2,128)S(1)}, u32[]{:S(2)}, u32[]{:S(2)}) async-start(f32[1,128,4,2,128]{4,3,2,0,1:T(2,128)} %copy.160), calls=%async_computation | async-start | bytes 1048576 | tf_op jit(solution)/shard_map/all_to_all | solution.py:132
  124.7 67.9 %reduce-scatter.2.cloned.1.call-start = ((), (), s32[]{:S(2)}) async-start(), calls=%async_computation.4 | async-start | bytes 163840 | tf_op jit(solution)/shard_map/reduce_scatter | solution.py:155
  133.7 6.1 %copy-start.14 = (f32[4]{0:T(128)S(1)}, f32[4]{0:T(128)}, u32[]{:S(2)}) copy-start(f32[4]{0:T(128)} %param.18) | copy-start | bytes 52
  133.7 6.4 %copy-start.9 = (f32[512]{0:T(512)S(1)}, f32[512]{0:T(512)}, u32[]{:S(2)}) copy-start(f32[512]{0:T(512)} %get-tuple-element.42) | copy-start | bytes 6148
  133.7 6.4 %copy-start.10 = (f32[512]{0:T(512)S(1)}, f32[512]{0:T(512)}, u32[]{:S(2)}) copy-start(f32[512]{0:T(512)} %get-tuple-element.43) | copy-start | bytes 6148
  133.7 37.3 %copy-start.3 = (bf16[512,512]{1,0:T(8,128)(2,1)S(1)}, bf16[512,512]{1,0:T(8,128)(2,1)}, u32[]{:S(2)}) copy-start(bf16[512,512]{1,0:T(8,128)(2,1)} %param.20) | copy-start | bytes 1572868
Sparse Core Ops, SparseCore 0:
  14.3 78.4 all-reduce.2
  172.0 20.4 reduce-scatter.1
where the time goes:
time: 200 us; the launch traced here: 199 us
  waiting for transfers between devices  60.8 us (30%)
  blocking collectives  54.5 us (27%)
  local copies, waits for them, and re-layouts  27.1 us (14%)
  matrix products  22.2 us (11%)
  between operations  14.5 us (7%)
  starting transfers between devices  13.1 us (7%)
  other arithmetic  7.19 us (4%)
    psum x1, waiting for transfers between devices, body(): lax.psum((part_query, part_key, part_value, squares_local), 'kv')  44.8 us
    all_gather x1, blocking collectives, body(): normed = lax.all_gather(finished, 'kv', axis=0, tiled=True)  30.8 us
    psum x1, blocking collectives, body(): lax.psum((part_query, part_key, part_value, squares_local), 'kv')  23.6 us
    unnamed x45, local copies, waits for them, and re-layouts  21.6 us
    reduce_scatter x1, waiting for transfers between devices, body(): lax.psum_scatter(jnp.dot(normed, w_out, preferred_element_type=jnp.float3...  11.8 us
    all_to_all x1, starting transfers between devices, body(): lax.all_to_all(leading(cache_part[0], token_count), 'kv', split_axis=1, c...  5.43 us
    dot_general x2, matrix products, softmax_block(): jnp.einsum('bjhmp,bphd->bjhmd', weights.astype(jnp.bfloat16), values, pre...  4.32 us
  transfers between devices with their start and end apart: 5, of which 4 were waited for; matrix products, arithmetic and copies ran while one was open for 21% of the time, Pallas kernels for 0%

commit v1 on v0

v1 whole, which is shorter than its diff:
```python
import functools

import jax
import jax.numpy as jnp
from jax import lax
from jax.experimental import pallas as pl
from jax.experimental.pallas import tpu as pltpu
from jax.sharding import PartitionSpec as P

KDIM = 128
HEAD = 64
PROP = 16

eps_row = 1e-06
eps_head = 1e-05
masked = -1e30
floor_max = -1e29

MESH = pl.DeviceIdType.MESH
VMEM = pl.BlockSpec(memory_space=pltpu.VMEM)
ANY = pl.BlockSpec(memory_space=pl.ANY)
SMEM = pl.BlockSpec(memory_space=pltpu.SMEM)
NT = (((1,), (1,)), ((), ()))
f32 = jnp.float32
bf16 = jnp.bfloat16


def iota(shape, dim):
    return lax.broadcasted_iota(jnp.int32, shape, dim)


def remote(src, dst, send, recv, **where):
    return pltpu.make_async_remote_copy(
        src_ref=src, dst_ref=dst, send_sem=send, recv_sem=recv, device_id=where, device_id_type=MESH
    )


def arrived(ref, send, recv, **where):
    remote(ref, ref, send, recv, **where).wait_recv()


def pair_rows(queries, heads):
    lane = iota((PROP, KDIM), 1)
    columns = [queries[:, h * KDIM : (h + 1) * KDIM].astype(f32) * (HEAD ** (-0.5)) for h in range(heads)]
    rows = [jnp.where(lane < HEAD, c, 0.0) for c in columns]
    rows += [jnp.where(lane >= HEAD, c, 0.0) for c in columns]
    return jnp.concatenate(rows, axis=0).astype(bf16)


def head_rows(array, heads):
    return jnp.concatenate([array[:, h * KDIM : (h + 1) * KDIM] for h in range(heads)], axis=0)


def stat_rows(maxima, totals):
    rows = maxima.shape[0]
    lane = iota((rows, KDIM), 1)
    wide = jnp.where(lane == 0, maxima, jnp.where(lane == 1, totals, 0.0))
    if rows < KDIM:
        wide = jnp.concatenate([wide, jnp.ones((KDIM - rows, KDIM), f32)], axis=0)
    return wide.T[:8, :]


def tree_part(own_queries, fresh, parent_row, heads):
    columns = heads * KDIM
    queries = pair_rows(own_queries, heads)
    keys = head_rows(fresh[:, :columns], heads)
    values = head_rows(fresh[:, columns:], heads)
    below = iota((PROP, PROP), 0)
    reach = jnp.logical_or(parent_row == below, below == iota((PROP, PROP), 1)).astype(f32)
    for repeat in range(max(1, (PROP - 1).bit_length())):
        narrow = reach.astype(bf16)
        reach = jnp.minimum(jnp.dot(narrow, narrow, preferred_element_type=f32), 1.0)
    rows, cols = 2 * heads * PROP, heads * PROP
    pick = (lax.rem(iota((rows, PROP), 0), PROP) == iota((rows, PROP), 1)).astype(bf16)
    spread = (lax.rem(iota((PROP, cols), 1), PROP) == iota((PROP, cols), 0)).astype(bf16)
    picked = lax.dot_general(pick, reach.astype(bf16), NT, preferred_element_type=f32)
    related = jnp.dot(picked.astype(bf16), spread, preferred_element_type=f32) > 0.5
    same = lax.rem(iota((rows, cols), 0) // PROP, heads) == iota((rows, cols), 1) // PROP
    s = lax.dot_general(queries, keys, NT, preferred_element_type=f32)
    allowed = jnp.logical_and(related, same)
    s = jnp.where(allowed, s, masked)
    top = jnp.max(s, axis=1, keepdims=True)
    w = jnp.where(allowed, jnp.exp(s - top), 0.0)
    total = jnp.sum(w, axis=1, keepdims=True)
    return top, total, jnp.dot(w.astype(bf16), values, preferred_element_type=f32)


def layer_kernel(n, n_tp, x_ref, gain_ref, wq_hbm, wk_hbm, wv_hbm, lam_ref, head_gain_ref, wo_hbm, ck_hbm, cv_hbm, len_ref, acc_ref, parents_ref,
                 out_ref, fresh_ref, *scratch):
    (w_in, wo, keys, values, part, send_q, send_k, send_v, recv_q, recv_k, recv_v, queries, scale, head_bias,
     scores_a, scores_b, weights_a, weights_b, sums, stats, got, got_stats, shares, normed, parts, got_parts,
     w_sem, c_sem, rs_s, rs_r, q_s, q_r, f_s, f_r, x_s, x_r, g_s, g_r, p_s, p_r) = scratch
    me = lax.axis_index("kv")
    tp = lax.axis_index("tp")
    sequences, rows_block, _ = ck_hbm.shape
    features, columns = wq_hbm.shape
    heads = columns // KDIM
    rows = 2 * heads * PROP
    positions = rows_block // heads
    group = n // sequences
    mine = me // group
    own = lax.rem(me, group) == 0
    barrier = pltpu.get_barrier_semaphore()
    for o in range(1, n):
        pl.semaphore_signal(barrier, inc=1, device_id={"kv": lax.rem(me + o, n)}, device_id_type=MESH)
    for o in range(1, n_tp):
        pl.semaphore_signal(barrier, inc=1, device_id={"tp": lax.rem(tp + o, n_tp)}, device_id_type=MESH)

    def when_own(run):
        if group > 1:
            pl.when(own)(run)
        else:
            run()

    def when_foreign(run):
        if group > 1:
            pl.when(jnp.logical_not(own))(run)

    def turn(o):
        return lax.rem(mine + o, sequences)

    local = [pltpu.make_async_copy(h, w_in.at[k], w_sem.at[k]) for k, h in enumerate((wq_hbm, wk_hbm, wv_hbm))]
    for copy in local:
        copy.start()

    def cached(k, b):
        return pltpu.make_async_copy((ck_hbm, cv_hbm)[k].at[b], (keys, values)[k].at[b], c_sem.at[k, b])

    for o in range(sequences):
        for k in range(2):
            cached(k, turn(o)).start()
    w_out_copy = pltpu.make_async_copy(wo_hbm, wo, w_sem.at[3])
    w_out_copy.start()

    wide = x_ref[...].astype(f32)
    scaled = (wide * gain_ref[...]).astype(bf16)
    squares = wide * wide
    folded = squares[:, :KDIM]
    for c in range(KDIM, features, KDIM):
        folded = folded + squares[:, c : c + KDIM]
    first_columns = columns + KDIM
    starts = (0, first_columns, first_columns + columns)
    sends, recvs = (send_q, send_k, send_v), (recv_q, recv_k, recv_v)
    part[:, :, columns:first_columns] = folded.reshape(sequences, PROP, KDIM)
    send_q[:, :, columns:] = folded.astype(bf16).reshape(sequences, PROP, KDIM)

    def project(k):
        local[k].wait()
        product = jnp.dot(scaled, w_in[k], preferred_element_type=f32)
        part[:, :, starts[k] : starts[k] + columns] = product.reshape(sequences, PROP, columns)
        sends[k][:, :, :columns] = product.astype(bf16).reshape(sequences, PROP, columns)

    def scatter(k, o):
        b = turn(o)
        return remote(sends[k].at[b], recvs[k].at[me], rs_s.at[k, b], rs_r.at[k, me], kv=b * group)

    def scatter_all(k):
        for o in range(1, sequences):
            scatter(k, o).start()
        when_foreign(lambda: scatter(k, 0).start())

    def summed(k, width):
        total = part[mine, :, starts[k] : starts[k] + width]
        for o in range(1, n):
            source = lax.rem(me + n - o, n)
            arrived(recvs[k].at[source], rs_s.at[k, 0], rs_r.at[k, source], kv=source)
            total = total + recvs[k][source].astype(f32)
        return total

    def spread(ref, send, recv):
        return [remote(ref.at[mine], ref.at[mine], send.at[o], recv.at[mine], kv=lax.rem(me + o, n)) for o in range(1, n)]

    def gathered(ref, send, recv, b):
        arrived(ref.at[b], send.at[0], recv.at[b], kv=b * group)

    project(0)
    pl.semaphore_wait(barrier, n - 1 + n_tp - 1)
    scatter_all(0)
    project(1)
    scatter_all(1)
    project(2)

    lane_head = lax.rem(iota((8, rows_block), 1), heads)
    for h in range(heads):
        head_bias[h] = jnp.where(lane_head == h, 0.0, masked)

    def finish_queries():
        total = summed(0, first_columns)
        mean = jnp.sum(total[:, columns:], axis=1, keepdims=True) / (features * n)
        inverse = lax.rsqrt(mean + eps_row)
        scale[...] = jnp.broadcast_to(inverse, scale.shape)
        queries[mine] = (inverse * total[:, :columns]).astype(bf16)
        for copy in spread(queries, q_s, q_r):
            copy.start()

    when_own(finish_queries)
    scatter_all(2)

    column = iota((8, rows_block), 1)

    def exchange(b):
        return (
            remote(sums.at[b], got.at[me], x_s.at[0, b], x_r.at[0, me], kv=b * group),
            remote(stats.at[b], got_stats.at[me], x_s.at[1, b], x_r.at[1, me], kv=b * group),
        )

    def attend(i, carry):
        two = (2 * i, 2 * i + 1)
        places = [turn(o) for o in two]
        for o, b in zip(two, places):
            for k in range(2):
                cached(k, b).wait()

            @pl.when(jnp.logical_or(o > 0, jnp.logical_not(own)))
            def _():
                gathered(queries, q_s, q_r, b)
        scored, weighed = (scores_a, scores_b), (weights_a, weights_b)
        for b, s_ref in zip(places, scored):
            s_ref[...] = lax.dot_general(pair_rows(queries[b], heads), keys[b], NT, preferred_element_type=f32)
        for b, s_ref, w_ref in zip(places, scored, weighed):
            limit = len_ref[b] + acc_ref[b] - me * positions
            beyond = jnp.where(column < limit * heads, 0.0, masked)
            maxima, totals = [None] * (2 * heads), [None] * (2 * heads)
            for h in range(heads):
                bias = head_bias[h] + beyond
                bias = jnp.concatenate([bias, bias], axis=0)
                for m in range(2):
                    r = m * heads + h
                    s = s_ref[r * PROP : (r + 1) * PROP, :] + bias
                    top = jnp.maximum(jnp.max(s, axis=1, keepdims=True), floor_max)
                    w = jnp.exp(s - top)
                    w_ref[r * PROP : (r + 1) * PROP, :] = w.astype(bf16)
                    maxima[r] = top
                    totals[r] = jnp.sum(w, axis=1, keepdims=True)
            sums[b] = jnp.dot(w_ref[...], values[b], preferred_element_type=f32).astype(bf16)
            stats[b] = stat_rows(jnp.concatenate(maxima, axis=0), jnp.concatenate(totals, axis=0))
        for o, b in zip(two, places):
            @pl.when(jnp.logical_or(o > 0, jnp.logical_not(own)))
            def _():
                for copy in exchange(b):
                    copy.start()
        return carry

    lax.fori_loop(0, sequences // 2, attend, 0)

    def finish_fresh():
        for k in (1, 2):
            fresh_ref[mine, :, (k - 1) * columns : k * columns] = (scale[:, :1] * summed(k, columns)).astype(bf16)
        for copy in spread(fresh_ref, f_s, f_r):
            copy.start()

    when_own(finish_fresh)

    def finish():
        top, total, tree_sums = tree_part(queries[mine], fresh_ref[mine], parents_ref[pl.ds(mine, 1), :], heads)
        tree = stat_rows(top, total)
        got_stats[me] = stats[mine]
        for o in range(1, n):
            source = lax.rem(me + n - o, n)
            arrived(got_stats.at[source], x_s.at[1, 0], x_r.at[1, source], kv=source)
        highest = tree[0:1]
        for s in range(n):
            highest = jnp.maximum(highest, got_stats[s, 0:1, :])
        tree_share = jnp.exp(tree[0:1] - highest)
        bottom = tree_share * tree[1:2]
        factors = []
        for s in range(n):
            factors.append(jnp.exp(got_stats[s, 0:1, :] - highest))
            bottom = bottom + factors[s] * got_stats[s, 1:2, :]
        shares[...] = jnp.zeros_like(shares)
        for s in range(n):
            shares[s : s + 1, :] = factors[s] / bottom
        shares[n : n + 1, :] = tree_share / bottom
        turned = shares[...].T[:rows]
        attended = turned[:, n : n + 1] * tree_sums
        got[me] = sums[mine]
        for o in range(1, n):
            source = lax.rem(me + n - o, n)
            arrived(got.at[source], x_s.at[0, 0], x_r.at[0, source], kv=source)
        for s in range(n):
            attended = attended + turned[:, s : s + 1] * got[s].astype(f32)
        half = rows // 2
        for h in range(heads):
            first = attended[h * PROP : (h + 1) * PROP]
            second = attended[half + h * PROP : half + (h + 1) * PROP]
            blended = first - lam_ref[h] * second
            mean = jnp.mean(blended * blended, axis=1, keepdims=True)
            value = (blended * lax.rsqrt(mean + eps_head) * head_gain_ref[...]).astype(bf16)
            normed[mine, :, h * KDIM : (h + 1) * KDIM] = value
        for copy in spread(normed, g_s, g_r):
            copy.start()

    when_own(finish)
    w_out_copy.wait()
    for o in range(1, sequences):
        gathered(normed, g_s, g_r, turn(o))
    when_foreign(lambda: gathered(normed, g_s, g_r, mine))
    everything = normed[...].reshape(sequences * PROP, columns)
    product = jnp.dot(everything, wo[...], preferred_element_type=f32)
    parts[...] = product.astype(bf16).reshape(parts.shape)

    def partial(o):
        to = lax.rem(tp + o, n_tp)
        return remote(parts.at[to], got_parts.at[tp], p_s.at[o], p_r.at[tp], tp=to)

    for o in range(1, n_tp):
        partial(o).start()
    for o in range(1, sequences):
        gathered(fresh_ref, f_s, f_r, turn(o))
    when_foreign(lambda: gathered(fresh_ref, f_s, f_r, mine))

    def sent(b):
        for copy in exchange(b):
            copy.wait_send()

    for o in range(1, sequences):
        for k in range(3):
            scatter(k, o).wait_send()
        sent(turn(o))

    def foreign_drain():
        for k in range(3):
            scatter(k, 0).wait_send()
        sent(mine)

    when_foreign(foreign_drain)

    def drain():
        for copy in spread(queries, q_s, q_r) + spread(fresh_ref, f_s, f_r) + spread(normed, g_s, g_r):
            copy.wait_send()

    when_own(drain)
    total = parts[tp].astype(f32)
    for o in range(1, n_tp):
        source = lax.rem(tp + n_tp - o, n_tp)
        arrived(got_parts.at[source], p_s.at[0], p_r.at[source], tp=source)
        total = total + got_parts[source].astype(f32)
    out_ref[...] = total.astype(bf16)
    for o in range(1, n_tp):
        partial(o).wait_send()


def place_kernel(heads, len_ref, acc_ref, fresh_ref, k_hbm, v_hbm, ko_hbm, vo_hbm, keys, values, in_sem, out_sem):
    sequences, rows_block, _ = k_hbm.shape
    columns = heads * KDIM
    positions = rows_block // heads
    start = lax.axis_index("kv") * positions
    sources, held, targets = (k_hbm, v_hbm), (keys, values), (ko_hbm, vo_hbm)

    def load(b, k):
        return pltpu.make_async_copy(sources[k].at[b], held[k].at[b], in_sem.at[k, b])

    def store(b, k):
        return pltpu.make_async_copy(held[k].at[b], targets[k].at[b], out_sem.at[k, b])

    every = [(b, k) for b in range(sequences) for k in range(2)]
    for b, k in every:
        load(b, k).start()
    window = (heads + 1) * PROP
    cols = heads * PROP
    row0 = iota((window, cols), 0)
    col = iota((window, cols), 1)
    wanted = lax.rem(col, PROP) * heads + col // PROP
    slot0 = iota((window, KDIM), 0)
    waiting = None
    for b, k in every:
        first = (len_ref[b] + acc_ref[b] - start) * heads
        base = jnp.clip((first // 16) * 16, 0, rows_block - window)
        base = pl.multiple_of(base, 16)
        placing = (row0 + (base - first) == wanted).astype(bf16)
        slot = slot0 + (base - first)
        written = jnp.logical_and(slot >= 0, slot < cols)
        fresh = head_rows(fresh_ref[b, :, k * columns : (k + 1) * columns], heads)
        placed = jnp.dot(placing, fresh, preferred_element_type=f32)
        load(b, k).wait()
        old = held[k][b, pl.ds(base, window), :].astype(f32)
        held[k][b, pl.ds(base, window), :] = jnp.where(written, placed, old).astype(bf16)
        if waiting is not None:
            store(*waiting).start()
        waiting = (b, k)
    store(*waiting).start()
    for b, k in every:
        store(b, k).wait()


def body(n, n_tp, tokens, norm_gain, w_query, w_key, w_value, lambdas, head_gain, w_out, cache_keys, cache_values, lengths, accepted, parents):
    sequences, positions, heads, _ = cache_keys.shape
    count, features = tokens.shape
    columns = heads * KDIM
    rows = 2 * heads * PROP
    block = positions * heads
    dma = pltpu.SemaphoreType.DMA
    flat = (sequences, block, KDIM)
    flat_keys, flat_values = cache_keys.reshape(flat), cache_values.reshape(flat)
    out_rows, out_columns = count // n_tp, w_out.shape[1]
    first_columns = columns + KDIM
    layer_out, fresh = pl.pallas_call(
        functools.partial(layer_kernel, n, n_tp),
        out_shape=(
            jax.ShapeDtypeStruct((out_rows, out_columns), bf16),
            jax.ShapeDtypeStruct((sequences, PROP, 2 * columns), bf16),
        ),
        in_specs=[VMEM, VMEM, ANY, ANY, ANY, SMEM, VMEM, ANY, ANY, ANY, SMEM, SMEM, VMEM],
        out_specs=(VMEM, VMEM),
        scratch_shapes=[
            pltpu.VMEM((3, features, columns), bf16),
            pltpu.VMEM(w_out.shape, bf16),
            pltpu.VMEM(flat, bf16),
            pltpu.VMEM(flat, bf16),
            pltpu.VMEM((sequences, PROP, 3 * columns + KDIM), f32),
            pltpu.VMEM((sequences, PROP, first_columns), bf16),
            pltpu.VMEM((sequences, PROP, columns), bf16),
            pltpu.VMEM((sequences, PROP, columns), bf16),
            pltpu.VMEM((n, PROP, first_columns), bf16),
            pltpu.VMEM((n, PROP, columns), bf16),
            pltpu.VMEM((n, PROP, columns), bf16),
            pltpu.VMEM((sequences, PROP, columns), bf16),
            pltpu.VMEM((PROP, KDIM), f32),
            pltpu.VMEM((heads, 8, block), f32),
            pltpu.VMEM((rows, block), f32),
            pltpu.VMEM((rows, block), f32),
            pltpu.VMEM((rows, block), bf16),
            pltpu.VMEM((rows, block), bf16),
            pltpu.VMEM((sequences, rows, KDIM), bf16),
            pltpu.VMEM((sequences, 8, KDIM), f32),
            pltpu.VMEM((n, rows, KDIM), bf16),
            pltpu.VMEM((n, 8, KDIM), f32),
            pltpu.VMEM((KDIM, KDIM), f32),
            pltpu.VMEM((sequences, PROP, columns), bf16),
            pltpu.VMEM((n_tp, out_rows, out_columns), bf16),
            pltpu.VMEM((n_tp, out_rows, out_columns), bf16),
            dma((4,)),
            dma((2, sequences)),
            dma((3, sequences)),
            dma((3, n)),
            dma((n,)),
            dma((sequences,)),
            dma((n,)),
            dma((sequences,)),
            dma((2, sequences)),
            dma((2, n)),
            dma((n,)),
            dma((sequences,)),
            dma((n_tp,)),
            dma((n_tp,)),
        ],
        compiler_params=pltpu.CompilerParams(collective_id=0, has_side_effects=True),
        name="layer",
    )(tokens, norm_gain.reshape(1, features), w_query, w_key, w_value, lambdas, head_gain.reshape(1, KDIM), w_out,
      flat_keys, flat_values, lengths, accepted, parents)

    keys_out, values_out = pl.pallas_call(
        functools.partial(place_kernel, heads),
        out_shape=(jax.ShapeDtypeStruct(flat, bf16), jax.ShapeDtypeStruct(flat, bf16)),
        in_specs=[SMEM, SMEM, VMEM, ANY, ANY],
        out_specs=(ANY, ANY),
        scratch_shapes=[
            pltpu.VMEM(flat, bf16),
            pltpu.VMEM(flat, bf16),
            dma((2, sequences)),
            dma((2, sequences)),
        ],
        name="place",
    )(lengths, accepted, fresh, flat_keys, flat_values)
    return (layer_out, keys_out.reshape(cache_keys.shape), values_out.reshape(cache_values.shape))


def solution(mesh):
    return jax.shard_map(
        functools.partial(body, mesh.shape["kv"], mesh.shape["tp"]),
        mesh=mesh,
        in_specs=(
            P(None, "kv"),
            P("kv"),
            P("kv", "tp"),
            P("kv", "tp"),
            P("kv", "tp"),
            P("tp"),
            P(),
            P("tp", "kv"),
            P(None, "kv", "tp", None),
            P(None, "kv", "tp", None),
            P(),
            P(),
            P(),
        ),
        out_specs=(P("tp", "kv"), P(None, "kv", "tp", None), P(None, "kv", "tp", None)),
        check_vma=False,
    )
```

time: 200 us -> 51.5 us (0.26)
  waiting for transfers between devices: 60.8 us -> 0 us
  blocking collectives: 54.5 us -> 0 us
  Pallas kernels: 0 us -> 50.1 us
  local copies, waits for them, and re-layouts: 27.1 us -> 0.62 us
  matrix products: 22.2 us -> 0 us
  between operations: 14.5 us -> 0.67 us
  starting transfers between devices: 13.1 us -> 0 us
  other arithmetic: 7.19 us -> 0 us
    pallas_call x0 -> x2, Pallas kernels: none -> 50.1 us  [the longest x1 42.6 us: body(): pl.pallas_call(functools.partial(layer_kernel, n, n_tp), out_shape=(jax.S...]
    psum x1 -> x0, waiting for transfers between devices: 44.8 us -> none  [body(): lax.psum((part_query, part_key, part_value, squares_local), 'kv')]
    all_gather x1 -> x0, blocking collectives: 30.8 us -> none  [body(): normed = lax.all_gather(finished, 'kv', axis=0, tiled=True)]
    psum x1 -> x0, blocking collectives: 23.6 us -> none  [body(): lax.psum((part_query, part_key, part_value, squares_local), 'kv')]
    dot_general x14 -> x0, matrix products: 22.2 us -> none  [the longest x2 4.32 us: softmax_block(): jnp.einsum('bjhmp,bphd->bjhmd', weights.astype(jnp.bfloat16), values, pre...]
    unnamed x45 -> x3, local copies, waits for them, and re-layouts: 21.6 us -> 0.62 us
    all_to_all x3 -> x0, starting transfers between devices: 12.8 us -> none  [the longest x1 5.43 us: body(): lax.all_to_all(leading(cache_part[0], token_count), 'kv', split_axis=1, c...]
    reduce_scatter x1 -> x0, waiting for transfers between devices: 11.8 us -> none  [body(): lax.psum_scatter(jnp.dot(normed, w_out, preferred_element_type=jnp.float3...]
  transfers between devices with their start and end apart: 5 -> 0, of which waited for: 4 -> 0; matrix products, arithmetic and copies ran while one was open for 21% -> 0% of each run, Pallas kernels for 0% -> 0%
where the time goes in v1:
time: 51.5 us; the launch traced here: 51.3 us
  Pallas kernels  50.1 us (97%)
  between operations  0.67 us (1%)
  local copies, waits for them, and re-layouts  0.62 us (1%)
    pallas_call x1, Pallas kernels, body(): pl.pallas_call(functools.partial(layer_kernel, n, n_tp), out_shape=(jax.S...  42.6 us
    pallas_call x1, Pallas kernels, body(): pl.pallas_call(functools.partial(place_kernel, heads), out_shape=(jax.Sha...  7.47 us

profile of v1, /device:TPU:0, one launch (start us, length us, event | category | flops | bytes accessed | tf_op | source)
XLA Modules:
  0.0 51.3 jit_solution(3728981495734262964)
XLA Ops:
  0.6 42.6 %layer.1 = (bf16[32,512]{1,0:T(8,128)(2,1)}, bf16[8,16,1024]{2,1,0:T(8,128)(2,1)}) custom-call(bf16[128,512]{1,0:T(8,128)(2,1)} %x_ref.1, f32[1,512]{1,0:T(1,128)} %bitcast.10, bf16[512,512]{1,0:T(8,128)(2,1)} %wq_hbm.1, bf16[512,512]{1,0:T(8,128)(2,1)} %wk_hbm.1, bf16[512,512]{1,0:T(8,128)(2,1)} %wv_hbm.1, f32[4]{0:T(128)} %lam_ref.1, f32[1,128]{1,0:T(1,128)} %bitcast.11, ...), custom_call_target="tpu_custom_call" | custom-call | tf_op jit(solution)/shard_map/layer/pallas_call | solution.py:397
  43.2 0.0 copy-start
  43.2 7.5 %place.1 = (bf16[8,2048,128]{2,1,0:T(8,128)(2,1)}, bf16[8,2048,128]{2,1,0:T(8,128)(2,1)}) custom-call(s32[8]{0:T(128)} %len_ref.3, s32[8]{0:T(128)} %acc_ref.3, bf16[8,16,1024]{2,1,0:T(8,128)(2,1)} %get-tuple-element.8.fresh_ref, bf16[8,2048,128]{2,1,0:T(8,128)(2,1)} %bitcast.7, bf16[8,2048,128]{2,1,0:T(8,128)(2,1)} %bitcast.9), custom_call_target="tpu_custom_call" | custom-call | tf_op jit(solution)/shard_map/place/pallas_call | solution.py:452
  50.7 0.0 copy-done
  50.7 0.6 %copy.17 = bf16[32,512]{1,0:T(8,128)(2,1)} copy(bf16[32,512]{1,0:T(8,128)(2,1)S(1)} %copy-done) | data formatting | bytes 65536
Async XLA Ops:
  43.2 7.5 %copy-start = (bf16[32,512]{1,0:T(8,128)(2,1)S(1)}, bf16[32,512]{1,0:T(8,128)(2,1)}, u32[]{:S(2)}) copy-start(bf16[32,512]{1,0:T(8,128)(2,1)} %get-tuple-element.14) | copy-start | bytes 98308
